TPU v7x, 256 devices: a whole 4x4x8 slice. The times are simulated.
256 devices in a mesh: ep: 64 (over z, y, core), tp: 4 (over x).
Axes of the slice: x: 4, y: 4, z: 8, core: 2. Of those that a mesh axis runs over, the one named last changes fastest.
Arguments:
- queries: bfloat16 [12288, 8, 128], P('ep', 'tp'), may hold values from -140 to 140
- keys: bfloat16 [12288, 4, 128], P('ep', 'tp'), may hold values from -6 to 6
- values: bfloat16 [12288, 4, 128], P('ep', 'tp'), may hold values from -6 to 6
- mix_scale: float32 [8], P('tp'), may hold values from 0.3 to 0.8
- head_gain: float32 [128], replicated, may hold values from 0.1 to 1.9
- out_weight: bfloat16 [8, 128, 2048], P('tp'), may hold values from -0.1875 to 0.1875
- moe_input: bfloat16 [24576, 2048], P(('ep', 'tp')), may hold values from -6 to 6
- norm_gain: float32 [2048], replicated, may hold values from 0.1 to 1.9
- routes: int32 [24576, 2], P(('ep', 'tp')), may hold values from 0 to 63, all different within a row; in each aligned block of 96 rows (0 to 95, 96 to 191, ...) at most 4 rows name the same one
- route_weights: float32 [24576, 2], P(('ep', 'tp')), may hold values from 0.2 to 1
- gate_weight: bfloat16 [64, 2048, 3584], P('ep', None, 'tp'), may hold values from -0.125 to 0.125
- up_weight: bfloat16 [64, 2048, 3584], P('ep', None, 'tp'), may hold values from -0.125 to 0.125
- down_weight: bfloat16 [64, 3584, 2048], P('ep', 'tp'), may hold values from -0.09375 to 0.09375
Outputs:
- attn_out: bfloat16 [12288, 2048], P(('ep', 'tp'))
- moe_out: bfloat16 [24576, 2048], P(('ep', 'tp'))
Inputs may be any that keep to these rules, and one draw needn't show every extreme that they name: `routes`: the 2 experts of a row differ. In each aligned block of 96 rows (the rows of one device) no expert is named by more than 4 rows, and in some blocks an expert is named by exactly 4 rows.
All inputs are finite; a program needn't handle non-finite values.
Results may differ from a plain program's by a relative error of at most 0.014.
Values may be sent and summed in bfloat16 or wider, within the bound.
A program may use at most 128 MiB of HBM per device.

v0:
```python
import math
import jax
import jax.numpy as jnp
from jax import lax
from jax.sharding import Mesh
from jax.sharding import PartitionSpec as P

EP = ("ep_0", "ep_1", "ep_2")
EP_TP = ("ep_0", "ep_1", "ep_2", "tp")
NEG_LARGE = -1e30


def joined_along(tiles, dim):
    tiles = jnp.moveaxis(tiles, 0, dim)
    lengths = tiles.shape
    return tiles.reshape(*lengths[:dim], lengths[dim] * lengths[dim + 1], *lengths[dim + 2 :])


def gather_in_order(value, axes, order):
    tiles = value[None]
    for k in order:
        tiles = lax.all_gather(tiles, axes[k], axis=0, tiled=True)
    current = [lax.axis_size(axes[k]) for k in reversed(order)]
    tiles = tiles.reshape(*current, *value.shape)
    turned = sorted(range(len(order)), key=lambda place: order[len(order) - 1 - place])
    return tiles.transpose(*turned, *range(len(order), tiles.ndim)).reshape(-1, *value.shape)


def gathered_by_axis(value, axes, order, dim):
    return joined_along(gather_in_order(value, axes, order), dim)


def split_up(value, dim, peers):
    before, after = (value.shape[:dim], value.shape[dim + 1 :])
    return jnp.moveaxis(value.reshape(*before, peers, -1, *after), dim, 0)


def summed_on_arrival(value, axis, dim):
    peers = lax.axis_size(axis)
    tiles = lax.all_to_all(split_up(value, dim, peers), axis, 0, 0, tiled=True)
    return jnp.sum(tiles.astype(jnp.float32), axis=0)


def attend_update(running, query_set, positions, key_block, value_block, key_anchor, scaling):
    row_peak, totals, numerator = running
    span = key_block.shape[0]
    scores = (
        jnp.einsum("tkgmd,skmd->kgmts", query_set, key_block, preferred_element_type=jnp.float32)
        * scaling
    )
    visible = (key_anchor + jnp.arange(span, dtype=jnp.int32))[None, :] <= positions[:, None]
    scores = jnp.where(visible, scores, NEG_LARGE)
    new_peak = jnp.maximum(row_peak, jnp.max(scores, axis=-1))
    weights = jnp.where(visible, jnp.exp(scores - new_peak[..., None]), 0.0)
    factor = jnp.exp(row_peak - new_peak)
    totals = totals * factor + jnp.sum(weights, axis=-1)
    numerator = numerator * factor[..., None] + jnp.einsum(
        "rnouf,frj->rnouj",
        weights.astype(jnp.bfloat16),
        value_block,
        preferred_element_type=jnp.float32,
    )
    return (new_peak, totals, numerator)


def body(
    queries,
    keys,
    values,
    mix_scale,
    head_gain,
    out_weight,
    moe_input,
    norm_gain,
    routes,
    route_weights,
    gate_weight,
    up_weight,
    down_weight,
):
    rows_here = queries.shape[0]
    key_heads = keys.shape[1]
    head_count = queries.shape[1]
    group_size = head_count // key_heads
    head_dim = queries.shape[2] // 2
    value_dim = values.shape[2]
    ep_size = lax.axis_size(EP)
    own_start = lax.axis_index(EP) * rows_here
    grouped = queries.reshape(rows_here, key_heads, group_size, 2, head_dim)
    own_positions = own_start + jnp.arange(rows_here, dtype=jnp.int32)
    query_sets = ((grouped, own_positions),)
    scaling = 1.0 / math.sqrt(head_dim)

    def empty_state(row_total):
        return (
            jnp.full((key_heads, group_size, 2, row_total), NEG_LARGE, jnp.float32),
            jnp.zeros((key_heads, group_size, 2, row_total), jnp.float32),
            jnp.zeros((key_heads, group_size, 2, row_total, value_dim), jnp.float32),
        )

    initial = tuple((empty_state(entry[0].shape[0]) for entry in query_sets))
    key_rows = gathered_by_axis(keys, EP, (1, 0, 2), 0)
    value_rows = gathered_by_axis(values, EP, (1, 0, 2), 0)
    length = key_rows.shape[0]
    span = length
    while span > 1024 and span % 2 == 0:
        span = span // 2
    key_rows = key_rows.reshape(length, key_heads, 2, head_dim)

    def sweep(step_id, states):
        anchor = step_id * span
        key_block = lax.dynamic_slice_in_dim(key_rows, step_id * span, span, 0)
        value_block = lax.dynamic_slice_in_dim(value_rows, step_id * span, span, 0)
        updated = []
        for (query_set, positions), status in zip(query_sets, states):

            def advance(current):
                return attend_update(
                    current, query_set, positions, key_block, value_block, anchor, scaling
                )

            def unchanged(current):
                return current

            updated.append(lax.cond(anchor <= positions[-1], advance, unchanged, status))
        return tuple(updated)

    folded = lax.fori_loop(0, length // span, sweep, initial)
    mixing = mix_scale.reshape(key_heads, group_size, 1, 1)
    outputs = []
    for status in folded:
        row_peak, totals, numerator = status
        blended = numerator[:, :, 0] / totals[:, :, 0, :, None] - mixing * (
            numerator[:, :, 1] / totals[:, :, 1, :, None]
        )
        normed = (
            blended
            * lax.rsqrt(jnp.mean(blended * blended, axis=-1, keepdims=True) + 1e-05)
            * head_gain
        )
        outputs.append(
            jnp.transpose(normed.astype(jnp.bfloat16), (2, 0, 1, 3)).reshape(
                -1, head_count * value_dim
            )
        )
    head_flat = outputs[0]
    weight_flat = out_weight.reshape(head_count * value_dim, -1)
    widened = moe_input.astype(jnp.float32)
    normed_in = (
        widened * lax.rsqrt(jnp.mean(widened * widened, axis=-1, keepdims=True) + 1e-06) * norm_gain
    ).astype(jnp.bfloat16)
    tok_count = moe_input.shape[0]
    top_count = routes.shape[1]
    experts = ep_size * gate_weight.shape[0]
    capacity = max(2, 3 * top_count * tok_count // (2 * experts))
    flattened = routes.reshape(-1)
    one_hot = (flattened[:, None] == jnp.arange(experts, dtype=jnp.int32)[None, :]).astype(
        jnp.int32
    )
    before = jnp.cumsum(one_hot, axis=0) - one_hot
    ranking = jnp.sum(before * one_hot, axis=1)
    slot_ids = (flattened * capacity + ranking).reshape(tok_count, top_count)
    slot_total = experts * capacity
    dispatch = jnp.any(
        jnp.arange(slot_total, dtype=jnp.int32)[:, None, None] == slot_ids[None], axis=2
    ).astype(jnp.bfloat16)
    outbound = jnp.dot(dispatch, normed_in, preferred_element_type=jnp.float32).astype(jnp.bfloat16)
    received = lax.all_to_all(outbound, EP, split_axis=0, concat_axis=0, tiled=True)
    inputs = lax.all_gather(received, "tp", axis=0, tiled=True)
    gate_proj = jnp.dot(inputs, gate_weight[0], preferred_element_type=jnp.float32)
    up_proj = jnp.dot(inputs, up_weight[0], preferred_element_type=jnp.float32)
    hidden_all = (jax.nn.silu(gate_proj) * up_proj).astype(jnp.bfloat16)
    attn_out = summed_on_arrival(
        jnp.dot(head_flat, weight_flat, preferred_element_type=jnp.float32).astype(jnp.bfloat16),
        "tp",
        0,
    ).astype(jnp.bfloat16)
    expert_out = summed_on_arrival(
        jnp.dot(hidden_all, down_weight[0], preferred_element_type=jnp.float32).astype(
            jnp.bfloat16
        ),
        "tp",
        0,
    ).astype(jnp.bfloat16)
    returned_rows = lax.all_to_all(expert_out, EP, split_axis=0, concat_axis=0, tiled=True)
    picked = jnp.take(returned_rows, slot_ids, axis=0)
    moe_out = jnp.sum(route_weights[:, :, None] * picked.astype(jnp.float32), axis=1).astype(
        jnp.bfloat16
    )
    return (attn_out, moe_out)


def solution(mesh):
    split = Mesh(mesh.devices.reshape(8, 4, 2, mesh.shape["tp"]), ("ep_0", "ep_1", "ep_2", "tp"))
    placed = (
        P(EP, "tp", None),
        P(EP, "tp", None),
        P(EP, "tp", None),
        P("tp"),
        P(),
        P("tp", None, None),
        P(EP_TP, None),
        P(),
        P(EP_TP, None),
        P(EP_TP, None),
        P(EP, None, "tp"),
        P(EP, None, "tp"),
        P(EP, "tp", None),
    )
    return jax.shard_map(
        body,
        mesh=split,
        in_specs=placed,
        out_specs=(P(EP_TP, None), P(EP_TP, None)),
        check_vma=False,
    )
```

profile of v0, /device:TPU:1, one launch (start us, length us, event | category | flops | bytes accessed | tf_op | source)
XLA Modules:
  0.0 368.3 jit_solution(15211746906782629320)
XLA Ops:
  7.2 12.6 %all-gather = bf16[768,1,128]{2,0,1:T(8,128)(2,1)} all-gather(bf16[192,1,128]{2,0,1:T(8,128)(2,1)} %param.18), channel_id=2, replica_groups=mesh['ep_0'=8,'ep_1'=4,'ep_2'=2,'tp'=4] {'ep_1'}, dimensions={0}, use_global_device_ids=true | all-gather | bytes 245760 | tf_op jit(solution)/shard_map/all_gather | solution.py:22
  19.9 10.2 %all-gather.1 = bf16[768,1,128]{2,0,1:T(8,128)(2,1)} all-gather(bf16[192,1,128]{2,0,1:T(8,128)(2,1)} %param.19), channel_id=3, replica_groups=mesh['ep_0'=8,'ep_1'=4,'ep_2'=2,'tp'=4] {'ep_1'}, dimensions={0}, use_global_device_ids=true | all-gather | bytes 245760 | tf_op jit(solution)/shard_map/all_gather | solution.py:22
  30.2 0.8 copy.86
  31.0 0.1 eq.35
  31.1 0.6 reduce-window.6
  31.7 0.2 slice_reduce_fusion
  32.1 0.1 reduce_sum.76
  32.3 0.7 compare_and_fusion
  33.1 1.2 fusion.22
  34.3 1.5 convolution_convert_fusion.1
  35.8 0.4 all_to_all.23
  36.3 47.2 %all_to_all.34 = bf16[64,4,2048]{2,1,0:T(4,128)(2,1)S(1)} all-to-all(bf16[64,4,2048]{2,1,0:T(4,128)(2,1)S(1)} %all_to_all.23), channel_id=1, replica_groups=mesh['ep_0'=8,'ep_1'=4,'ep_2'=2,'tp'=4] {'ep_0','ep_1','ep_2'}, dimensions={0} | all-to-all | bytes 2097152 | tf_op jit(solution)/shard_map/all_to_all | solution.py:168
  83.5 1.1 all_to_all.25
  84.7 0.5 all-gather.10.cloned.1.call-update
  85.2 23.4 %all-gather.12.cloned.1.call-done = bf16[32,192,1,128]{3,1,2,0:T(8,128)(2,1)} async-done(((bf16[4,192,1,128]{3,1,2,0:T(8,128)(2,1)}), bf16[32,192,1,128]{3,1,2,0:T(8,128)(2,1)}) %all-gather.12.cloned.1.call-update) | async-done | bytes 1572880 | tf_op jit(solution)/shard_map/all_gather | solution.py:22
  108.7 54.8 %all-gather.16.cloned.1.call-done = bf16[1024,2048]{1,0:T(8,128)(2,1)} async-done(((bf16[256,2048]{1,0:T(8,128)(2,1)}), bf16[1024,2048]{1,0:T(8,128)(2,1)}) %all-gather.16.cloned.1.call-update) | async-done | bytes 4194320 | tf_op jit(solution)/shard_map/all_gather | solution.py:169
  163.5 7.5 %fusion.16 = f32[1024,896]{1,0:T(8,128)S(1)} fusion(bf16[1024,2048]{1,0:T(8,128)(2,1)} %all-gather.16.cloned.1.call-done, bf16[1,2048,896]{2,1,0:T(8,128)(2,1)} %param.28), kind=kOutput, calls=%fused_computation.26 | convolution fusion | flops 3758096384 | bytes 11534336 | tf_op jit(solution)/shard_map/dot_general | solution.py:171
  171.0 4.7 %multiply_convert_fusion = bf16[1024,896]{1,0:T(8,128)(2,1)S(1)} fusion(f32[1024,896]{1,0:T(8,128)S(1)} %fusion.16, bf16[1024,2048]{1,0:T(8,128)(2,1)S(1)} %copy-done.5, bf16[1,2048,896]{2,1,0:T(8,128)(2,1)S(1)} %copy-done.6), kind=kOutput, calls=%fused_computation.30 | convolution fusion | flops 3763601408 | bytes 13369344 | tf_op jit(solution)/shard_map/dot_general | solution.py:170
  175.8 6.1 %convolution_convert_fusion = bf16[1024,2048]{1,0:T(8,128)(2,1)} fusion(bf16[1024,896]{1,0:T(8,128)(2,1)S(1)} %multiply_convert_fusion, bf16[1,896,2048]{2,1,0:T(8,128)(2,1)S(1)} %copy-done.7), kind=kOutput, calls=%fused_computation.24 | convolution fusion | flops 3760193536 | bytes 9699328 | tf_op jit(solution)/shard_map/dot_general | solution.py:179
  181.9 5.1 %all-to-all-start.2 = ((bf16[4,256,2048]{2,1,0:T(8,128)(2,1)}), bf16[4,256,2048]{2,1,0:T(8,128)(2,1)}, u32[]{:S(2)}, u32[]{:S(2)}) async-start(bf16[4,256,2048]{2,1,0:T(8,128)(2,1)} %bitcast.121), calls=%async_computation.2 | async-start | bytes 8388608 | tf_op jit(solution)/shard_map/all_to_all | solution.py:40
  187.1 0.1 copy.80
  187.2 11.2 %copy.79 = bf16[8,4,2,192,1,128]{3,2,1,0,5,4:T(2,128)(2,1)} copy(bf16[8,4,2,192,1,128]{5,3,1,0,2,4:T(8,128)(2,1)} %bitcast.122) | data formatting | bytes 6291456 | tf_op jit(solution)/shard_map/transpose | solution.py:26
  198.4 9.9 %reshape_reshape_reshape.3 = bf16[12288,1,2,64]{0,3,2,1:T(8,128)(2,1)} reshape(bf16[8,4,2,192,1,128]{3,2,1,0,5,4:T(2,128)(2,1)} %copy.79) | data formatting | bytes 6291456 | tf_op jit(solution)/shard_map/reshape;reshape;reshape | solution.py:108
  208.4 3.9 %copy.81 = bf16[8,4,2,192,1,128]{5,3,2,1,0,4:T(8,128)(2,1)} copy(bf16[8,4,2,192,1,128]{5,3,1,0,2,4:T(8,128)(2,1)} %bitcast.124) | data formatting | bytes 6291456 | tf_op jit(solution)/shard_map/transpose | solution.py:26
  212.3 24.4 %while.17 = (s32[]{:T(128)}, f32[1,2,2,192]{3,1,2,0:T(2,128)S(1)}, f32[1,2,2,192]{3,1,2,0:T(2,128)S(1)}, f32[1,2,2,192,128]{4,3,2,1,0:T(8,128)S(1)}, s32[192]{0:...) while((s32[]{:T(128)}, f32[1,2,2,192]{3,1,2,0:T(2,128)S(1)}, ...), condition=%wide.region_5.6_spmd, body=%wide.region_0.5_spmd.sunk | while | flops 232147968 | bytes 8857645 | solution.py:128
  212.4 0.6 slice.57
  213.6 4.3 %conditional.2 = ((f32[1,2,2,192]{3,1,2,0:T(2,128)S(1)}, f32[1,2,2,192]{3,1,2,0:T(2,128)S(1)}, f32[1,2,2,192,128]{4,3,2,1,0:T(8,128)S(1)})) conditional(s32[]{:T(128)} %convert_element_type.91, (f32[1,2,2,192]{3,1,2,0:T(2,128)S(1)}, f32[1,2,2,192]{3,1,2,0:T(2,128)S(1)}, f32[1,2,2,192,128]{4,3,2,1,0:T(8,128)S(1)}) %tuple.61, (s32[]{:T(128)}, ...), branch_computations={%region_1.0_spmd, %region_2.4_spmd} | conditional | flops 232147968 | bytes 8857422 | solution.py:125
  213.6 0.1 broadcast_compare_fusion
  213.8 1.6 fusion
  215.4 0.9 fusion.4
  216.3 1.5 fusion.3
  217.9 0.6 slice.57
  219.1 0.6 slice.57
  220.4 0.6 slice.57
  221.7 0.6 slice.57
  222.9 0.6 slice.57
  224.2 0.6 slice.57
  225.4 0.6 slice.57
  226.7 0.6 slice.57
  227.9 0.6 slice.57
  229.2 0.6 slice.57
  230.4 0.6 slice.57
  231.7 0.6 slice.57
  233.0 0.6 slice.57
  234.2 0.6 slice.57
  235.5 0.6 slice.57
  236.7 0.3 multiply_reduce_fusion.1
  237.1 0.1 fusion.32
  237.3 1.3 convolution_convert_fusion.2
  238.6 4.0 %all-to-all-start = ((bf16[4,48,2048]{2,1,0:T(8,128)(2,1)}), bf16[4,48,2048]{2,1,0:T(8,128)(2,1)S(1)}, u32[]{:S(2)}, u32[]{:S(2)}) async-start(bf16[4,48,2048]{2,1,0:T(8,128)(2,1)} %bitcast.30), calls=%async_computation | async-start | bytes 1572864 | tf_op jit(solution)/shard_map/all_to_all | solution.py:40
  242.6 3.1 reduce_sum.78
  245.7 1.2 all_to_all.27
  246.9 6.6 %all-to-all-done = bf16[4,48,2048]{2,1,0:T(8,128)(2,1)S(1)} async-done(((bf16[4,48,2048]{2,1,0:T(8,128)(2,1)}), bf16[4,48,2048]{2,1,0:T(8,128)(2,1)S(1)}, u32[]{:S(2)}, u32[]{:S(2)}) %all-to-all-start) | async-done | bytes 786464 | tf_op jit(solution)/shard_map/all_to_all | solution.py:40
  253.5 74.0 %all-to-all-start.3 = ((bf16[64,4,2048]{2,1,0:T(4,128)(2,1)}), bf16[64,4,2048]{2,1,0:T(4,128)(2,1)S(1)}, u32[]{:S(2)}, u32[]{:S(2)}) async-start(bf16[64,4,2048]{2,1,0:T(4,128)(2,1)} %all_to_all.27), calls=%async_computation.3 | async-start | bytes 2097152 | tf_op jit(solution)/shard_map/all_to_all | solution.py:185
  327.5 0.1 copy.91
  327.6 0.1 reshape.218
  327.7 0.1 copy.90
  327.9 0.1 copy.85
  328.0 0.8 reduce_sum.74
  328.8 26.8 %all-to-all-done.3 = bf16[64,4,2048]{2,1,0:T(4,128)(2,1)S(1)} async-done(((bf16[64,4,2048]{2,1,0:T(4,128)(2,1)}), bf16[64,4,2048]{2,1,0:T(4,128)(2,1)S(1)}, u32[]{:S(2)}, u32[]{:S(2)}) %all-to-all-start.3) | async-done | bytes 1048608 | tf_op jit(solution)/shard_map/all_to_all | solution.py:185
  355.6 0.3 all_to_all.29
  355.9 1.1 gather_fusion
  357.1 0.5 reshape.217
  357.6 4.2 %multiply_reduce_fusion = bf16[96,2048]{1,0:T(8,128)(2,1)} fusion(bf16[96,2,2048]{2,1,0:T(2,128)(2,1)S(1)} %reshape.217, pred[96,2]{1,0:T(8,128)(4,1)S(1)} %copy.90, f32[96,2]{1,0:T(8,128)S(1)} %copy.85), kind=kLoop, calls=%fused_computation.33 | loop fusion | flops 1376256 | bytes 1180608 | tf_op jit(solution)/shard_map/reduce_sum | solution.py:187
  (68 shorter events, 1.1 us)
Async XLA Ops:
  7.2 230.1 %copy-start = (bf16[2,128,2048]{2,1,0:T(8,128)(2,1)S(1)}, bf16[2,128,2048]{2,1,0:T(8,128)(2,1)}, u32[]{:S(2)}) copy-start(bf16[2,128,2048]{2,1,0:T(8,128)(2,1)} %param.22) | copy-start | bytes 3145732
  7.2 77.5 %all-gather.8.cloned.1.call-start = ((), (), s32[]{:S(2)}) async-start(), calls=%async_computation.4 | async-start | bytes 1769472 | tf_op jit(solution)/shard_map/all_gather | solution.py:22
  19.9 88.8 %all-gather.12.cloned.1.call-start = ((), (), s32[]{:S(2)}) async-start(), calls=%async_computation.6 | async-start | bytes 1769472 | tf_op jit(solution)/shard_map/all_gather | solution.py:22
  30.1 133.4 %all-gather.16.cloned.1.call-start = ((), (), s32[]{:S(2)}) async-start(), calls=%async_computation.8 | async-start | bytes 5242880 | tf_op jit(solution)/shard_map/all_gather | solution.py:169
  84.6 102.6 %all-gather.10.cloned.1.call-start = ((), (), s32[]{:S(2)}) async-start(), calls=%async_computation.5 | async-start | bytes 4718592 | tf_op jit(solution)/shard_map/all_gather | solution.py:22
  85.2 123.2 %all-gather.14.cloned.1.call-start = ((), (), s32[]{:S(2)}) async-start(), calls=%async_computation.7 | async-start | bytes 4718592 | tf_op jit(solution)/shard_map/all_gather | solution.py:22
  163.5 7.5 %copy-start.5 = (bf16[1024,2048]{1,0:T(8,128)(2,1)S(1)}, bf16[1024,2048]{1,0:T(8,128)(2,1)}, u32[]{:S(2)}) copy-start(bf16[1024,2048]{1,0:T(8,128)(2,1)} %all-gather.16.cloned.1.call-done) | copy-start | bytes 12582916
  163.5 7.5 %copy-start.6 = (bf16[1,2048,896]{2,1,0:T(8,128)(2,1)S(1)}, bf16[1,2048,896]{2,1,0:T(8,128)(2,1)}, u32[]{:S(2)}) copy-start(bf16[1,2048,896]{2,1,0:T(8,128)(2,1)} %param.27) | copy-start | bytes 11010052
  171.0 4.8 %copy-start.7 = (bf16[1,896,2048]{2,1,0:T(8,128)(2,1)S(1)}, bf16[1,896,2048]{2,1,0:T(8,128)(2,1)}, u32[]{:S(2)}) copy-start(bf16[1,896,2048]{2,1,0:T(8,128)(2,1)} %param.29) | copy-start | bytes 11010052
  181.9 5.2 %copy-start.1 = (bf16[192,2,128]{2,1,0:T(2,128)(2,1)S(1)}, bf16[192,2,128]{2,1,0:T(2,128)(2,1)}, u32[]{:S(2)}) copy-start(bf16[192,2,128]{2,1,0:T(2,128)(2,1)} %param.17) | copy-start | bytes 294916
  181.9 56.7 %all-to-all-start.2 = ((bf16[4,256,2048]{2,1,0:T(8,128)(2,1)}), bf16[4,256,2048]{2,1,0:T(8,128)(2,1)}, u32[]{:S(2)}, u32[]{:S(2)}) async-start(bf16[4,256,2048]{2,1,0:T(8,128)(2,1)} %bitcast.121), calls=%async_computation.2 | async-start | bytes 8388608 | tf_op jit(solution)/shard_map/all_to_all | solution.py:40
  212.3 24.4 %copy-start.4 = (f32[2]{0:T(128)S(1)}, f32[2]{0:T(128)}, u32[]{:S(2)}) copy-start(f32[2]{0:T(128)} %param.20) | copy-start | bytes 28
  212.3 24.7 %copy-start.3 = (f32[128]{0:T(128)S(1)}, f32[128]{0:T(128)}, u32[]{:S(2)}) copy-start(f32[128]{0:T(128)} %param.21) | copy-start | bytes 1540
  238.6 14.9 %all-to-all-start = ((bf16[4,48,2048]{2,1,0:T(8,128)(2,1)}), bf16[4,48,2048]{2,1,0:T(8,128)(2,1)S(1)}, u32[]{:S(2)}, u32[]{:S(2)}) async-start(bf16[4,48,2048]{2,1,0:T(8,128)(2,1)} %bitcast.30), calls=%async_computation | async-start | bytes 1572864 | tf_op jit(solution)/shard_map/all_to_all | solution.py:40
  245.7 82.2 %copy-start.2 = (f32[96,2]{0,1:T(2,128)S(1)}, f32[96,2]{0,1:T(2,128)}, u32[]{:S(2)}) copy-start(f32[96,2]{0,1:T(2,128)} %param.26) | copy-start | bytes 2308
  253.5 102.2 %all-to-all-start.3 = ((bf16[64,4,2048]{2,1,0:T(4,128)(2,1)}), bf16[64,4,2048]{2,1,0:T(4,128)(2,1)S(1)}, u32[]{:S(2)}, u32[]{:S(2)}) async-start(bf16[64,4,2048]{2,1,0:T(4,128)(2,1)} %all_to_all.27), calls=%async_computation.3 | async-start | bytes 2097152 | tf_op jit(solution)/shard_map/all_to_all | solution.py:185
Sparse Core Ops, SparseCore 0:
  20.0 43.5 all-gather.7
  65.3 43.2 all-gather.11
  110.5 52.9 all-gather.15
  165.2 18.7 all-gather.9
  185.6 18.7 all-gather.13
where the time goes:
time: 370 us; the launch traced here: 368 us
  waiting for transfers between devices  112 us (30%)
  starting transfers between devices  83.3 us (23%)
  blocking collectives  70 us (19%)
  local copies, waits for them, and re-layouts  41.2 us (11%)
  matrix products  24.3 us (7%)
  between operations  14.1 us (4%)
  other arithmetic  12.4 us (3%)
  loops' own time  10.7 us (3%)
    all_to_all x1, starting transfers between devices, body(): lax.all_to_all(expert_out, EP, split_axis=0, concat_axis=0, tiled=True)  74 us
    all_gather x1, waiting for transfers between devices, body(): inputs = lax.all_gather(received, 'tp', axis=0, tiled=True)  54.8 us
    all_to_all x1, blocking collectives, body(): lax.all_to_all(outbound, EP, split_axis=0, concat_axis=0, tiled=True)  47.2 us
    all_to_all x1, waiting for transfers between devices, body(): lax.all_to_all(expert_out, EP, split_axis=0, concat_axis=0, tiled=True)  26.8 us
    all_gather x4, waiting for transfers between devices, gather_in_order(): tiles = lax.all_gather(tiles, axes[k], axis=0, tiled=True)  23.5 us
    all_gather x2, blocking collectives, gather_in_order(): tiles = lax.all_gather(tiles, axes[k], axis=0, tiled=True)  22.8 us
    transpose x2, local copies, waits for them, and re-layouts, gather_in_order(): tiles.transpose(*turned, *range(len(order), tiles.ndim))  15.1 us
    another operation x1, loops' own time, body(): folded = lax.fori_loop(0, length // span, sweep, initial)  10.4 us
  transfers between devices with their start and end apart: 8, of which 4 were waited for; matrix products, arithmetic and copies ran while one was open for 19% of the time, Pallas kernels for 0%

commit v1 on v0

--- a/solution.py
+++ b/solution.py
@@ -1,3 +1,4 @@
+import functools
 import math
 import jax
 import jax.numpy as jnp
@@ -8,6 +9,16 @@
 EP = ("ep_0", "ep_1", "ep_2")
 EP_TP = ("ep_0", "ep_1", "ep_2", "tp")
 NEG_LARGE = -1e30
+
+
+def name_the_loads(s0, dimension_no):
+    low = jnp.concatenate(
+        lax.all_to_all(jnp.stack(lax.axis_size("tp") * [s0]), "tp", 0, 0), axis=dimension_no
+    )
+    return low
+
+
+see_samples = functools.partial(name_the_loads, dimension_no=0)
 
 
 def joined_along(tiles, dim):
@@ -166,7 +177,7 @@
     ).astype(jnp.bfloat16)
     outbound = jnp.dot(dispatch, normed_in, preferred_element_type=jnp.float32).astype(jnp.bfloat16)
     received = lax.all_to_all(outbound, EP, split_axis=0, concat_axis=0, tiled=True)
-    inputs = lax.all_gather(received, "tp", axis=0, tiled=True)
+    inputs = see_samples(received)
     gate_proj = jnp.dot(inputs, gate_weight[0], preferred_element_type=jnp.float32)
     up_proj = jnp.dot(inputs, up_weight[0], preferred_element_type=jnp.float32)
     hidden_all = (jax.nn.silu(gate_proj) * up_proj).astype(jnp.bfloat16)

time: 370 us -> 349 us (0.943)
  waiting for transfers between devices: 112 us -> 79.8 us
  local copies, waits for them, and re-layouts: 41.2 us -> 45.7 us
    all_gather x1 -> x0, waiting for transfers between devices: 54.8 us -> none  [body(): inputs = lax.all_gather(received, 'tp', axis=0, tiled=True)]
    all_to_all x0 -> x1, waiting for transfers between devices: none -> 31.9 us  [name_the_loads(): lax.all_to_all(jnp.stack(lax.axis_size('tp') * [s0]), 'tp', 0, 0)]
    all_gather x4, waiting for transfers between devices: 23.5 us -> 16.3 us  [gather_in_order(): tiles = lax.all_gather(tiles, axes[k], axis=0, tiled=True)]
    all_to_all x0 -> x1, starting transfers between devices: none -> 4.85 us  [name_the_loads(): lax.all_to_all(jnp.stack(lax.axis_size('tp') * [s0]), 'tp', 0, 0)]
    another operation x2 -> x4, local copies, waits for them, and re-layouts: 0.19 us -> 4.09 us  [the longest x2 3.9 us: name_the_loads(): jnp.stack(lax.axis_size('tp') * [s0])]
  transfers between devices with their start and end apart: 8 -> 8, of which waited for: 4 -> 4; matrix products, arithmetic and copies ran while one was open for 19% -> 22% of each run, Pallas kernels for 0% -> 0%
where the time goes in v1:
time: 349 us; the launch traced here: 347 us
  starting transfers between devices  86.3 us (25%)
  waiting for transfers between devices  79.8 us (23%)
  blocking collectives  70.1 us (20%)
  local copies, waits for them, and re-layouts  45.7 us (13%)
  matrix products  26.9 us (8%)
  between operations  14.1 us (4%)
  other arithmetic  13.5 us (4%)
  loops' own time  10.9 us (3%)
    all_to_all x1, starting transfers between devices, body(): lax.all_to_all(expert_out, EP, split_axis=0, concat_axis=0, tiled=True)  72.2 us
    all_to_all x1, blocking collectives, body(): lax.all_to_all(outbound, EP, split_axis=0, concat_axis=0, tiled=True)  47.3 us
    all_to_all x1, waiting for transfers between devices, name_the_loads(): lax.all_to_all(jnp.stack(lax.axis_size('tp') * [s0]), 'tp', 0, 0)  31.9 us
    all_to_all x1, waiting for transfers between devices, body(): lax.all_to_all(expert_out, EP, split_axis=0, concat_axis=0, tiled=True)  25.7 us
    all_gather x2, blocking collectives, gather_in_order(): tiles = lax.all_gather(tiles, axes[k], axis=0, tiled=True)  22.8 us
    all_gather x4, waiting for transfers between devices, gather_in_order(): tiles = lax.all_gather(tiles, axes[k], axis=0, tiled=True)  16.3 us
    transpose x2, local copies, waits for them, and re-layouts, gather_in_order(): tiles.transpose(*turned, *range(len(order), tiles.ndim))  15.1 us
    another operation x1, loops' own time, body(): folded = lax.fori_loop(0, length // span, sweep, initial)  10.7 us
  transfers between devices with their start and end apart: 8, of which 4 were waited for; matrix products, arithmetic and copies ran while one was open for 22% of the time, Pallas kernels for 0%

profile of v1, /device:TPU:1, one launch (start us, length us, event | category | flops | bytes accessed | tf_op | source)
XLA Modules:
  0.0 347.3 jit_solution(563593959831310710)
XLA Ops:
  7.2 12.6 %all-gather = bf16[768,1,128]{2,0,1:T(8,128)(2,1)} all-gather(bf16[192,1,128]{2,0,1:T(8,128)(2,1)} %param.18), channel_id=2, replica_groups=mesh['ep_0'=8,'ep_1'=4,'ep_2'=2,'tp'=4] {'ep_1'}, dimensions={0}, use_global_device_ids=true | all-gather | bytes 245760 | tf_op jit(solution)/shard_map/all_gather | solution.py:33
  19.9 10.2 %all-gather.1 = bf16[768,1,128]{2,0,1:T(8,128)(2,1)} all-gather(bf16[192,1,128]{2,0,1:T(8,128)(2,1)} %param.19), channel_id=3, replica_groups=mesh['ep_0'=8,'ep_1'=4,'ep_2'=2,'tp'=4] {'ep_1'}, dimensions={0}, use_global_device_ids=true | all-gather | bytes 245760 | tf_op jit(solution)/shard_map/all_gather | solution.py:33
  30.2 0.8 copy.86
  31.0 0.1 eq.35
  31.1 0.6 reduce-window.6
  31.7 0.2 slice_reduce_fusion
  32.1 0.1 reduce_sum.76
  32.3 0.7 compare_and_fusion
  33.1 1.2 fusion.22
  34.3 1.5 convolution_convert_fusion.1
  35.8 0.4 all_to_all.24
  36.3 47.3 %all_to_all.36 = bf16[64,4,2048]{2,1,0:T(4,128)(2,1)} all-to-all(bf16[64,4,2048]{2,1,0:T(4,128)(2,1)S(1)} %all_to_all.24), channel_id=1, replica_groups=mesh['ep_0'=8,'ep_1'=4,'ep_2'=2,'tp'=4] {'ep_0','ep_1','ep_2'}, dimensions={0} | all-to-all | bytes 2097152 | tf_op jit(solution)/shard_map/all_to_all | solution.py:179
  83.6 1.4 stack.4
  85.0 2.5 stack.10
  87.5 4.8 %all-to-all-start.2 = ((bf16[4,256,2048]{2,1,0:T(8,128)(2,1)}), bf16[4,256,2048]{2,1,0:T(8,128)(2,1)}, u32[]{:S(2)}, u32[]{:S(2)}) async-start(bf16[4,256,2048]{2,1,0:T(8,128)(2,1)} %stack.10), calls=%async_computation.2 | async-start | bytes 8388608 | tf_op jit(solution)/shard_map/all_to_all | solution.py:16
  92.4 16.2 %all-gather.11.cloned.1.call-done = bf16[32,192,1,128]{3,1,2,0:T(8,128)(2,1)} async-done(((bf16[4,192,1,128]{3,1,2,0:T(8,128)(2,1)}), bf16[32,192,1,128]{3,1,2,0:T(8,128)(2,1)}) %all-gather.11.cloned.1.call-update) | async-done | bytes 1572880 | tf_op jit(solution)/shard_map/all_gather | solution.py:33
  108.7 31.9 %all-to-all-done.2 = bf16[4,256,2048]{2,1,0:T(8,128)(2,1)} async-done(((bf16[4,256,2048]{2,1,0:T(8,128)(2,1)}), bf16[4,256,2048]{2,1,0:T(8,128)(2,1)}, u32[]{:S(2)}, u32[]{:S(2)}) %all-to-all-start.2) | async-done | bytes 4194336 | tf_op jit(solution)/shard_map/all_to_all | solution.py:16
  140.6 7.5 %fusion.16 = f32[1024,896]{1,0:T(8,128)S(1)} fusion(bf16[1024,2048]{1,0:T(8,128)(2,1)} %bitcast.32, bf16[1,2048,896]{2,1,0:T(8,128)(2,1)} %param.28), kind=kOutput, calls=%fused_computation.26 | convolution fusion | flops 3758096384 | bytes 11534336 | tf_op jit(solution)/shard_map/dot_general | solution.py:182
  148.1 7.3 %multiply_convert_fusion = bf16[1024,896]{1,0:T(8,128)(2,1)S(1)} fusion(f32[1024,896]{1,0:T(8,128)S(1)} %fusion.16, bf16[1024,2048]{1,0:T(8,128)(2,1)} %bitcast.32, bf16[1,2048,896]{2,1,0:T(8,128)(2,1)S(1)} %copy-done.6), kind=kOutput, calls=%fused_computation.30 | convolution fusion | flops 3763601408 | bytes 13369344 | tf_op jit(solution)/shard_map/dot_general | solution.py:181
  155.5 6.1 %convolution_convert_fusion = bf16[1024,2048]{1,0:T(8,128)(2,1)} fusion(bf16[1024,896]{1,0:T(8,128)(2,1)S(1)} %multiply_convert_fusion, bf16[1,896,2048]{2,1,0:T(8,128)(2,1)S(1)} %copy-done.7), kind=kOutput, calls=%fused_computation.24 | convolution fusion | flops 3760193536 | bytes 9699328 | tf_op jit(solution)/shard_map/dot_general | solution.py:190
  161.5 5.2 %all-to-all-start.3 = ((bf16[4,256,2048]{2,1,0:T(8,128)(2,1)}), bf16[4,256,2048]{2,1,0:T(8,128)(2,1)}, u32[]{:S(2)}, u32[]{:S(2)}) async-start(bf16[4,256,2048]{2,1,0:T(8,128)(2,1)} %bitcast.122), calls=%async_computation.3 | async-start | bytes 8388608 | tf_op jit(solution)/shard_map/all_to_all | solution.py:51
  166.7 0.1 copy.80
  166.9 11.1 %copy.79 = bf16[8,4,2,192,1,128]{3,2,1,0,5,4:T(2,128)(2,1)} copy(bf16[8,4,2,192,1,128]{5,3,1,0,2,4:T(8,128)(2,1)} %bitcast.123) | data formatting | bytes 6291456 | tf_op jit(solution)/shard_map/transpose | solution.py:37
  178.0 9.8 %reshape_reshape_reshape.3 = bf16[12288,1,2,64]{0,3,2,1:T(8,128)(2,1)} reshape(bf16[8,4,2,192,1,128]{3,2,1,0,5,4:T(2,128)(2,1)} %copy.79) | data formatting | bytes 6291456 | tf_op jit(solution)/shard_map/reshape;reshape;reshape | solution.py:119
  187.9 3.9 %copy.81 = bf16[8,4,2,192,1,128]{5,3,2,1,0,4:T(8,128)(2,1)} copy(bf16[8,4,2,192,1,128]{5,3,1,0,2,4:T(8,128)(2,1)} %bitcast.125) | data formatting | bytes 6291456 | tf_op jit(solution)/shard_map/transpose | solution.py:37
  191.9 25.5 %while.17 = (s32[]{:T(128)}, f32[1,2,2,192]{3,1,2,0:T(2,128)S(1)}, f32[1,2,2,192]{3,1,2,0:T(2,128)S(1)}, f32[1,2,2,192,128]{4,3,2,1,0:T(8,128)S(1)}, s32[192]{0:...) while((s32[]{:T(128)}, f32[1,2,2,192]{3,1,2,0:T(2,128)S(1)}, ...), condition=%wide.region_5.6_spmd, body=%wide.region_0.5_spmd.sunk | while | flops 232147968 | bytes 8857645 | solution.py:139
  191.9 0.6 slice.57
  193.2 4.3 %conditional.2 = ((f32[1,2,2,192]{3,1,2,0:T(2,128)S(1)}, f32[1,2,2,192]{3,1,2,0:T(2,128)S(1)}, f32[1,2,2,192,128]{4,3,2,1,0:T(8,128)S(1)})) conditional(s32[]{:T(128)} %convert_element_type.91, (f32[1,2,2,192]{3,1,2,0:T(2,128)S(1)}, f32[1,2,2,192]{3,1,2,0:T(2,128)S(1)}, f32[1,2,2,192,128]{4,3,2,1,0:T(8,128)S(1)}) %tuple.61, (s32[]{:T(128)}, ...), branch_computations={%region_1.0_spmd, %region_2.4_spmd} | conditional | flops 232147968 | bytes 8857422 | solution.py:136
  193.2 0.1 broadcast_compare_fusion
  193.4 1.6 fusion
  195.0 0.9 fusion.4
  195.9 1.5 fusion.3
  197.5 0.6 slice.57
  198.8 0.6 slice.57
  200.1 0.6 slice.57
  201.5 0.6 slice.57
  202.8 0.6 slice.57
  204.1 0.6 slice.57
  205.4 0.6 slice.57
  206.8 0.6 slice.57
  208.1 0.6 slice.57
  209.4 0.6 slice.57
  210.7 0.6 slice.57
  212.1 0.6 slice.57
  213.4 0.6 slice.57
  214.7 0.6 slice.57
  216.0 0.6 slice.57
  217.4 0.3 multiply_reduce_fusion.1
  217.7 0.1 fusion.32
  217.9 1.3 convolution_convert_fusion.2
  219.3 4.0 %all-to-all-start = ((bf16[4,48,2048]{2,1,0:T(8,128)(2,1)}), bf16[4,48,2048]{2,1,0:T(8,128)(2,1)S(1)}, u32[]{:S(2)}, u32[]{:S(2)}) async-start(bf16[4,48,2048]{2,1,0:T(8,128)(2,1)} %bitcast.30), calls=%async_computation | async-start | bytes 1572864 | tf_op jit(solution)/shard_map/all_to_all | solution.py:51
  223.3 3.1 reduce_sum.78
  226.3 1.2 all_to_all.28
  227.6 5.9 %all-to-all-done = bf16[4,48,2048]{2,1,0:T(8,128)(2,1)S(1)} async-done(((bf16[4,48,2048]{2,1,0:T(8,128)(2,1)}), bf16[4,48,2048]{2,1,0:T(8,128)(2,1)S(1)}, u32[]{:S(2)}, u32[]{:S(2)}) %all-to-all-start) | async-done | bytes 786464 | tf_op jit(solution)/shard_map/all_to_all | solution.py:51
  233.4 0.9 copy-done.1
  234.3 72.2 %all-to-all-start.4 = ((bf16[64,4,2048]{2,1,0:T(4,128)(2,1)}), bf16[64,4,2048]{2,1,0:T(4,128)(2,1)S(1)}, u32[]{:S(2)}, u32[]{:S(2)}) async-start(bf16[64,4,2048]{2,1,0:T(4,128)(2,1)} %all_to_all.28), calls=%async_computation.4 | async-start | bytes 2097152 | tf_op jit(solution)/shard_map/all_to_all | solution.py:196
  306.7 0.1 reshape.225
  306.8 0.1 copy.90
  307.0 2.0 reduce_sum.74
  309.0 25.7 %all-to-all-done.4 = bf16[64,4,2048]{2,1,0:T(4,128)(2,1)S(1)} async-done(((bf16[64,4,2048]{2,1,0:T(4,128)(2,1)}), bf16[64,4,2048]{2,1,0:T(4,128)(2,1)S(1)}, u32[]{:S(2)}, u32[]{:S(2)}) %all-to-all-start.4) | async-done | bytes 1048608 | tf_op jit(solution)/shard_map/all_to_all | solution.py:196
  334.7 0.3 all_to_all.30
  335.0 1.1 gather_fusion
  336.1 0.5 reshape.224
  336.6 4.2 %multiply_reduce_fusion = bf16[96,2048]{1,0:T(8,128)(2,1)} fusion(bf16[96,2,2048]{2,1,0:T(2,128)(2,1)S(1)} %reshape.224, pred[96,2]{1,0:T(8,128)(4,1)S(1)} %copy.90, f32[96,2]{1,0:T(8,128)S(1)} %copy.85), kind=kLoop, calls=%fused_computation.33 | loop fusion | flops 1376256 | bytes 1180608 | tf_op jit(solution)/shard_map/reduce_sum | solution.py:198
  (68 shorter events, 1.3 us)
Async XLA Ops:
  7.2 210.8 %copy-start = (bf16[2,128,2048]{2,1,0:T(8,128)(2,1)S(1)}, bf16[2,128,2048]{2,1,0:T(8,128)(2,1)}, u32[]{:S(2)}) copy-start(bf16[2,128,2048]{2,1,0:T(8,128)(2,1)} %param.22) | copy-start | bytes 3145732
  7.2 77.8 %all-gather.7.cloned.1.call-start = ((), (), s32[]{:S(2)}) async-start(), calls=%async_computation.5 | async-start | bytes 1769472 | tf_op jit(solution)/shard_map/all_gather | solution.py:33
  19.9 88.8 %all-gather.11.cloned.1.call-start = ((), (), s32[]{:S(2)}) async-start(), calls=%async_computation.7 | async-start | bytes 1769472 | tf_op jit(solution)/shard_map/all_gather | solution.py:33
  30.1 136.7 %all-gather.9.cloned.1.call-start = ((), (), s32[]{:S(2)}) async-start(), calls=%async_computation.6 | async-start | bytes 4718592 | tf_op jit(solution)/shard_map/all_gather | solution.py:33
  87.5 53.1 %all-to-all-start.2 = ((bf16[4,256,2048]{2,1,0:T(8,128)(2,1)}), bf16[4,256,2048]{2,1,0:T(8,128)(2,1)}, u32[]{:S(2)}, u32[]{:S(2)}) async-start(bf16[4,256,2048]{2,1,0:T(8,128)(2,1)} %stack.10), calls=%async_computation.2 | async-start | bytes 8388608 | tf_op jit(solution)/shard_map/all_to_all | solution.py:16
  92.4 95.5 %all-gather.13.cloned.1.call-start = ((), (), s32[]{:S(2)}) async-start(), calls=%async_computation.8 | async-start | bytes 4718592 | tf_op jit(solution)/shard_map/all_gather | solution.py:33
  140.6 7.5 %copy-start.6 = (bf16[1,2048,896]{2,1,0:T(8,128)(2,1)S(1)}, bf16[1,2048,896]{2,1,0:T(8,128)(2,1)}, u32[]{:S(2)}) copy-start(bf16[1,2048,896]{2,1,0:T(8,128)(2,1)} %param.27) | copy-start | bytes 11010052
  148.1 7.4 %copy-start.7 = (bf16[1,896,2048]{2,1,0:T(8,128)(2,1)S(1)}, bf16[1,896,2048]{2,1,0:T(8,128)(2,1)}, u32[]{:S(2)}) copy-start(bf16[1,896,2048]{2,1,0:T(8,128)(2,1)} %param.29) | copy-start | bytes 11010052
  161.5 5.2 %copy-start.2 = (bf16[192,2,128]{2,1,0:T(2,128)(2,1)S(1)}, bf16[192,2,128]{2,1,0:T(2,128)(2,1)}, u32[]{:S(2)}) copy-start(bf16[192,2,128]{2,1,0:T(2,128)(2,1)} %param.17) | copy-start | bytes 294916
  161.5 57.7 %all-to-all-start.3 = ((bf16[4,256,2048]{2,1,0:T(8,128)(2,1)}), bf16[4,256,2048]{2,1,0:T(8,128)(2,1)}, u32[]{:S(2)}, u32[]{:S(2)}) async-start(bf16[4,256,2048]{2,1,0:T(8,128)(2,1)} %bitcast.122), calls=%async_computation.3 | async-start | bytes 8388608 | tf_op jit(solution)/shard_map/all_to_all | solution.py:51
  191.8 25.5 %copy-start.5 = (f32[2]{0:T(128)S(1)}, f32[2]{0:T(128)}, u32[]{:S(2)}) copy-start(f32[2]{0:T(128)} %param.20) | copy-start | bytes 28
  191.9 25.8 %copy-start.4 = (f32[128]{0:T(128)S(1)}, f32[128]{0:T(128)}, u32[]{:S(2)}) copy-start(f32[128]{0:T(128)} %param.21) | copy-start | bytes 1540
  219.3 14.2 %all-to-all-start = ((bf16[4,48,2048]{2,1,0:T(8,128)(2,1)}), bf16[4,48,2048]{2,1,0:T(8,128)(2,1)S(1)}, u32[]{:S(2)}, u32[]{:S(2)}) async-start(bf16[4,48,2048]{2,1,0:T(8,128)(2,1)} %bitcast.30), calls=%async_computation | async-start | bytes 1572864 | tf_op jit(solution)/shard_map/all_to_all | solution.py:51
  226.3 80.6 %copy-start.3 = (f32[96,2]{0,1:T(2,128)S(1)}, f32[96,2]{0,1:T(2,128)}, u32[]{:S(2)}) copy-start(f32[96,2]{0,1:T(2,128)} %param.26) | copy-start | bytes 2308
  233.4 0.9 copy-start.1
  234.3 100.4 %all-to-all-start.4 = ((bf16[64,4,2048]{2,1,0:T(4,128)(2,1)}), bf16[64,4,2048]{2,1,0:T(4,128)(2,1)S(1)}, u32[]{:S(2)}, u32[]{:S(2)}) async-start(bf16[64,4,2048]{2,1,0:T(4,128)(2,1)} %all_to_all.28), calls=%async_computation.4 | async-start | bytes 2097152 | tf_op jit(solution)/shard_map/all_to_all | solution.py:196
Sparse Core Ops, SparseCore 0:
  20.0 43.5 all-gather.6
  65.3 43.2 all-gather.10
  110.5 20.5 all-gather.8
  132.7 18.7 all-gather.12
